TPU v7x, 32 devices: a whole 2x2x4 slice. The times are simulated.
32 devices in a mesh: fs: 16 (over z, y, x), tp: 2 (over core).
Axes of the slice: x: 2, y: 2, z: 4, core: 2. Of those that a mesh axis runs over, the one named last changes fastest.
Arguments:
- residual_in: bfloat16 [4096, 2048], P(('fs', 'tp')), may hold values from -6 to 6
- gain_first: float32 [2048], replicated, may hold values from 0.1 to 1.9
- gain_mixer: float32 [2048], replicated, may hold values from 0.1 to 1.9
- gain_second: float32 [2048], replicated, may hold values from 0.1 to 1.9
- gate_weight: float32 [2048, 6144], P('fs', 'tp'), may hold values from -0.125 to 0.125
- gate_scale: float32 [6144], P('tp'), may hold values from 0.3 to 3
- up_weight: float32 [2048, 6144], P('fs', 'tp'), may hold values from -0.125 to 0.125
- up_scale: float32 [6144], P('tp'), may hold values from 0.3 to 3
- down_weight: float32 [6144, 2048], P('tp', 'fs'), may hold values from -0.078125 to 0.078125
- down_scale: float32 [2048], P('fs'), may hold values from 0.3 to 3
- query_weight: float32 [2048, 2048], P('fs', 'tp'), may hold values from -0.125 to 0.125
- query_scale: float32 [2048], P('tp'), may hold values from 0.3 to 3
- key_weight: float32 [2048, 2048], P('fs', 'tp'), may hold values from -0.125 to 0.125
- key_scale: float32 [2048], P('tp'), may hold values from 0.3 to 3
- value_weight: float32 [2048, 2048], P('fs', 'tp'), may hold values from -0.125 to 0.125
- value_scale: float32 [2048], P('tp'), may hold values from 0.3 to 3
- output_weight: float32 [2048, 2048], P('tp', 'fs'), may hold values from -0.125 to 0.125
- output_scale: float32 [2048], P('fs'), may hold values from 0.3 to 3
Outputs:
- residual_out: bfloat16 [4096, 2048], P(('fs', 'tp'))
All inputs are finite; a program needn't handle non-finite values.
Results may differ from a plain program's by a relative error of at most 0.028.
Values may be sent and summed in bfloat16 or wider, within the bound.
A program may use at most 128 MiB of HBM per device.

v0:
```python
import jax
import jax.numpy as jnp
from jax import lax
from jax.sharding import PartitionSpec as P

HEADS = 8
HEAD_DIM = 256
BLOCK = 64
EPSILON = 1e-06
HEAD_FLOOR = 0.25
ROTARY_BASE = 10000.0
HIGHEST = lax.Precision.HIGHEST


def normalize(sequence_rows, gain_vector):
    values = sequence_rows.astype(jnp.float32)
    scaled = values * lax.rsqrt(jnp.mean(values * values, axis=-1, keepdims=True) + EPSILON)
    return (scaled * gain_vector).astype(jnp.bfloat16)


def collect_rows(sequence_rows, gain_vector):
    return lax.all_gather(normalize(sequence_rows, gain_vector), "tp", axis=0, tiled=True)


def return_rows(inputs, weight, factor):
    term = jnp.dot(inputs, weight, preferred_element_type=jnp.float32) * factor
    return lax.psum_scatter(
        lax.optimization_barrier(term.astype(jnp.bfloat16))
        .astype(jnp.float32)
        .astype(jnp.bfloat16),
        "tp",
        scatter_dimension=0,
        tiled=True,
    ).astype(jnp.float32)


def head_rates(first_head, head_count, length):
    head_number = (first_head + jnp.arange(head_count)).astype(jnp.float32)
    return jnp.exp(jnp.log(1.0 / 16.0) + head_number / (HEADS - 1) * jnp.log(4.0 / length))


def rotate(values, positions):
    half_width = values.shape[-1] // 2
    frequency = ROTARY_BASE ** (-jnp.arange(half_width, dtype=jnp.float32) * 2.0 / values.shape[-1])
    angles = positions[:, None] * frequency[None, :]
    cosine = jnp.cos(angles)[:, None, :]
    sine_value = jnp.sin(angles)[:, None, :]
    front_half = values[..., :half_width]
    back_half = values[..., half_width:]
    return jnp.concatenate(
        [
            front_half * cosine - back_half * sine_value,
            back_half * cosine + front_half * sine_value,
        ],
        axis=-1,
    )


def retention(query_pre, key_pre, value_pre, decay_rates):
    length, head_count, head_width = query_pre.shape
    positions = jnp.arange(length, dtype=jnp.float32)
    query_rot = rotate(query_pre, positions).astype(jnp.bfloat16)
    key_rot = rotate(key_pre, positions).astype(jnp.bfloat16)
    value_low = value_pre.astype(jnp.bfloat16)
    blocks = length // BLOCK
    inside = jnp.arange(BLOCK, dtype=jnp.float32)
    distance = inside[:, None] - inside[None, :]
    within = jnp.where(
        distance >= 0, jnp.exp(-decay_rates[:, None, None] * jnp.maximum(distance, 0.0)), 0.0
    ) * head_width ** (-0.5)
    query_blocks = query_rot.reshape(blocks, BLOCK, head_count, head_width)
    key_blocks = key_rot.reshape(blocks, BLOCK, head_count, head_width)
    value_blocks = value_low.reshape(blocks, BLOCK, head_count, head_width)
    scores = jnp.einsum(
        "nihe,njhe->nhij", query_blocks, key_blocks, preferred_element_type=jnp.float32
    )
    weights = (scores * within[None]).astype(jnp.bfloat16)
    inner_part = jnp.einsum(
        "nhij,njhe->nihe", weights, value_blocks, preferred_element_type=jnp.float32
    )
    fading = jnp.exp(-decay_rates[None, :] * (BLOCK - 1.0 - inside[:, None])) * head_width ** (-0.5)
    key_faded = key_blocks.astype(jnp.float32) * fading[None, :, :, None]
    updates = jnp.einsum(
        "njhd,njhe->nhde", key_faded, value_blocks.astype(jnp.float32), precision=HIGHEST
    )
    block_decay = jnp.exp(-decay_rates * BLOCK)

    def advance(memory_state, update):
        return (memory_state * block_decay[:, None, None] + update, memory_state)

    _, before = lax.scan(
        advance, jnp.zeros((head_count, head_width, head_width), jnp.float32), updates
    )
    rising = jnp.exp(-decay_rates[None, :] * (inside[:, None] + 1.0))
    queried = query_blocks.astype(jnp.float32) * rising[None, :, :, None]
    carried_part = jnp.einsum("nihd,nhde->nihe", queried, before, precision=HIGHEST)
    combined = (inner_part + carried_part).reshape(length, head_count, head_width)
    normed = combined * lax.rsqrt(
        jnp.maximum(jnp.mean(combined * combined, axis=-1, keepdims=True), HEAD_FLOOR)
    )
    return normed.astype(jnp.bfloat16).reshape(length, head_count * head_width)


def body(
    residual_in,
    gain_first,
    gain_mixer,
    gain_second,
    gate_weight,
    gate_scale,
    up_weight,
    up_scale,
    down_weight,
    down_scale,
    query_weight,
    query_scale,
    key_weight,
    key_scale,
    value_weight,
    value_scale,
    output_weight,
    output_scale,
):
    gate_part = gate_weight.astype(jnp.bfloat16)
    up_part = up_weight.astype(jnp.bfloat16)
    down_factor, output_factor = (
        lax.all_gather(down_scale, "fs", axis=0, tiled=True),
        lax.all_gather(output_scale, "fs", axis=0, tiled=True),
    )
    first_input = collect_rows(residual_in, gain_first)
    gate_full, up_full = (
        lax.all_gather(gate_part, "fs", axis=0, tiled=True),
        lax.all_gather(up_part, "fs", axis=0, tiled=True),
    )
    gate_pre = jnp.dot(first_input, gate_full, preferred_element_type=jnp.float32)
    up_pre = jnp.dot(first_input, up_full, preferred_element_type=jnp.float32)
    down_full = lax.all_gather(down_weight.astype(jnp.bfloat16), "fs", axis=1, tiled=True)
    hidden_first = (jax.nn.silu(gate_pre * gate_scale) * (up_pre * up_scale)).astype(jnp.bfloat16)
    mlp_first = return_rows(hidden_first, down_full, down_factor)
    middle = (residual_in.astype(jnp.float32) + 0.5 * mlp_first).astype(jnp.bfloat16)
    mixer_input = collect_rows(middle, gain_mixer)
    local_width = query_weight.shape[1]
    projections = (
        query_weight.astype(jnp.bfloat16),
        key_weight.astype(jnp.bfloat16),
        value_weight.astype(jnp.bfloat16),
    )
    pieces = (
        lax.all_gather(projections[0], "fs", axis=0, tiled=True),
        lax.all_gather(projections[1], "fs", axis=0, tiled=True),
        lax.all_gather(projections[2], "fs", axis=0, tiled=True),
    )
    query_pre, key_pre, value_pre = tuple(
        (
            jnp.dot(mixer_input, pieces[member], preferred_element_type=jnp.float32)
            for member in range(3)
        )
    )
    output_full = lax.all_gather(output_weight.astype(jnp.bfloat16), "fs", axis=1, tiled=True)
    length = mixer_input.shape[0]
    heads_local = local_width // HEAD_DIM
    decay_rates = head_rates(lax.axis_index("tp") * heads_local, heads_local, length)
    mixed = retention(
        (query_pre * query_scale).reshape(length, heads_local, HEAD_DIM),
        (key_pre * key_scale).reshape(length, heads_local, HEAD_DIM),
        (value_pre * value_scale).reshape(length, heads_local, HEAD_DIM),
        decay_rates,
    )
    mixer_out = return_rows(mixed, output_full, output_factor)
    second = (middle.astype(jnp.float32) + mixer_out).astype(jnp.bfloat16)
    last_input = collect_rows(second, gain_second)
    gate_last = jnp.dot(last_input, gate_full, preferred_element_type=jnp.float32) * gate_scale
    up_last = jnp.dot(last_input, up_full, preferred_element_type=jnp.float32) * up_scale
    hidden_second = (jax.nn.silu(gate_last) * up_last).astype(jnp.bfloat16)
    mlp_second = return_rows(hidden_second, down_full, down_factor)
    return (second.astype(jnp.float32) + 0.5 * mlp_second).astype(jnp.bfloat16)


def solution(mesh):
    in_specs = (
        P(("fs", "tp"), None),
        P(),
        P(),
        P(),
        P("fs", "tp"),
        P("tp"),
        P("fs", "tp"),
        P("tp"),
        P("tp", "fs"),
        P("fs"),
        P("fs", "tp"),
        P("tp"),
        P("fs", "tp"),
        P("tp"),
        P("fs", "tp"),
        P("tp"),
        P("tp", "fs"),
        P("fs"),
    )
    out_specs = P(("fs", "tp"), None)
    return jax.shard_map(body, mesh=mesh, in_specs=in_specs, out_specs=out_specs, check_vma=False)
```

profile of v0, /device:TPU:0, one launch (start us, length us, event | category | flops | bytes accessed | tf_op | source)
XLA Modules:
  0.0 955.4 jit_solution(6325975038016141110)
XLA Ops:
  16.0 43.0 %all-gather = f32[16,1,128]{2,1,0:T(1,128)S(1)} all-gather(f32[1,1,128]{2,1,0:T(1,128)S(1)} %bitcast.58), channel_id=1, replica_groups=mesh['fs'=16,'tp'=2] {'fs'}, dimensions={0}, use_global_device_ids=true | all-gather | bytes 8704 | tf_op jit(solution)/shard_map/all_gather | solution.py:127
  59.0 118.3 %all-gather.15.cloned.1.call-done = bf16[2048,3072]{1,0:T(8,128)(2,1)} async-done(((bf16[128,3072]{1,0:T(8,128)(2,1)}), bf16[2048,3072]{1,0:T(8,128)(2,1)}) %all-gather.15.cloned.1.call-update) | async-done | bytes 12582928 | tf_op jit(solution)/shard_map/all_gather | solution.py:132
  177.3 9.9 %convolution_multiply_fusion.3 = f32[256,3072]{1,0:T(8,128)} fusion(bf16[256,2048]{1,0:T(8,128)(2,1)} %all-gather.13.cloned.1.call-done, bf16[2048,3072]{1,0:T(8,128)(2,1)} %all-gather.15.cloned.1.call-done, f32[3072]{0:T(1024)S(1)} %copy-done.20), kind=kOutput, calls=%fused_computation.7 | convolution fusion | flops 3222011904 | bytes 16789504 | tf_op jit(solution)/shard_map/dot_general | solution.py:135
  187.2 142.5 %all-gather.17.cloned.1.call-done = bf16[2048,3072]{1,0:T(8,128)(2,1)} async-done(((bf16[128,3072]{1,0:T(8,128)(2,1)}), bf16[2048,3072]{1,0:T(8,128)(2,1)}) %all-gather.17.cloned.1.call-update) | async-done | bytes 12582928 | tf_op jit(solution)/shard_map/all_gather | solution.py:133
  329.7 196.2 %all-gather.19.cloned.1.call-done = bf16[3072,2048]{1,0:T(8,128)(2,1)} async-done(((bf16[3072,128]{1,0:T(8,128)(2,1)}), bf16[3072,2048]{1,0:T(8,128)(2,1)}) %all-gather.19.cloned.1.call-update) | async-done | bytes 12582928 | tf_op jit(solution)/shard_map/all_gather | solution.py:137
  525.9 17.1 %fusion.6 = bf16[256,2048]{1,0:T(8,128)(2,1)} fusion(bf16[3072,2048]{1,0:T(8,128)(2,1)} %all-gather.19.cloned.1.call-done, f32[2048]{0:T(1024)S(1)} %bitcast.56, bf16[256,2048]{1,0:T(8,128)(2,1)S(1)} %copy-done.18, bf16[2048,3072]{1,0:T(8,128)(2,1)} %all-gather.17.cloned.1.call-done, f32[256,3072]{1,0:T(8,128)} %convolution_multiply_fusion.3, ...), kind=kOutput, calls=%fused_computation.15 | convolution fusion | flops 6449004544 | bytes 30429184 | tf_op jit(solution)/shard_map/dot_general | solution.py:26
  544.0 5.9 reduce-scatter.4.cloned.1.call-done
  554.8 41.1 %all-gather.1 = f32[16,1,128]{2,1,0:T(1,128)S(1)} all-gather(f32[1,1,128]{2,1,0:T(1,128)S(1)} %bitcast.59), channel_id=1, replica_groups=mesh['fs'=16,'tp'=2] {'fs'}, dimensions={0}, use_global_device_ids=true | all-gather | bytes 8704 | tf_op jit(solution)/shard_map/all_gather | solution.py:128
  598.0 31.3 %all-gather.25.cloned.1.call-done = bf16[2048,1024]{1,0:T(8,128)(2,1)} async-done(((bf16[128,1024]{1,0:T(8,128)(2,1)}), bf16[2048,1024]{1,0:T(8,128)(2,1)}) %all-gather.25.cloned.1.call-update) | async-done | bytes 4194320 | tf_op jit(solution)/shard_map/all_gather | solution.py:149
  629.2 9.2 all-gather.21.cloned.1.call-done
  638.4 4.7 convolution_multiply_fusion.8
  644.9 73.1 %all-gather.27.cloned.1.call-done = bf16[2048,1024]{1,0:T(8,128)(2,1)} async-done(((bf16[128,1024]{1,0:T(8,128)(2,1)}), bf16[2048,1024]{1,0:T(8,128)(2,1)}) %all-gather.27.cloned.1.call-update) | async-done | bytes 4194320 | tf_op jit(solution)/shard_map/all_gather | solution.py:150
  718.0 4.7 convolution_multiply_fusion.7
  725.4 69.6 %all-gather.23.cloned.1.call-done = bf16[2048,1024]{1,0:T(8,128)(2,1)} async-done(((bf16[128,1024]{1,0:T(8,128)(2,1)}), bf16[2048,1024]{1,0:T(8,128)(2,1)}) %all-gather.23.cloned.1.call-update) | async-done | bytes 4194320 | tf_op jit(solution)/shard_map/all_gather | solution.py:151
  795.0 4.6 fusion.10
  806.7 10.4 %while.13 = (s32[]{:T(128)}, f32[4,256,256]{2,1,0:T(8,128)S(1)}, f32[4,4,256,256]{3,2,1,0:T(8,128)}, f32[4,4,256,256]{3,2,1,0:T(8,128)}, s32[]{:T(128)}, /*index=5*/s32[]{:T(128)}, s32[]{:T(128)}) while((s32[]{:T(128)}, f32[4,256,256]{2,1,0:T(8,128)S(1)}, f32[4,4,256,256]{3,2,1,0:T(8,128)}, f32[4,4,256,256]{3,2,1,0:T(8,128)}, ...), condition=%wide.region_4.5_spmd.clone, body=%wide.region_3.4_spmd.clone.sunk | while | flops 1048603 | bytes 5243520 | solution.py:91
  817.2 5.1 fusion.24
  825.5 59.4 %all-gather.29.cloned.1.call-done = bf16[1024,2048]{1,0:T(8,128)(2,1)} async-done(((bf16[1024,128]{1,0:T(8,128)(2,1)}), bf16[1024,2048]{1,0:T(8,128)(2,1)}) %all-gather.29.cloned.1.call-update) | async-done | bytes 4194320 | tf_op jit(solution)/shard_map/all_gather | solution.py:159
  884.9 4.5 fusion.8
  889.5 6.7 reduce-scatter.6.cloned.1.call-done
  899.9 10.1 %all-gather.31.cloned.1.call-done = bf16[256,2048]{1,0:T(8,128)(2,1)} async-done(((bf16[128,2048]{1,0:T(8,128)(2,1)}), bf16[256,2048]{1,0:T(8,128)(2,1)}) %all-gather.31.cloned.1.call-update) | async-done | bytes 1048592 | tf_op jit(solution)/shard_map/all_gather | solution.py:22
  909.9 10.0 %convolution_multiply_fusion.1 = f32[256,3072]{1,0:T(8,128)} fusion(bf16[256,2048]{1,0:T(8,128)(2,1)} %all-gather.31.cloned.1.call-done, bf16[2048,3072]{1,0:T(8,128)(2,1)} %all-gather.15.cloned.1.call-done, f32[3072]{0:T(1024)S(1)} %copy-done.21), kind=kOutput, calls=%fused_computation.5 | convolution fusion | flops 3222011904 | bytes 16789504 | tf_op jit(solution)/shard_map/dot_general | solution.py:172
  920.0 17.0 %fusion.7 = bf16[256,2048]{1,0:T(8,128)(2,1)} fusion(bf16[3072,2048]{1,0:T(8,128)(2,1)} %all-gather.19.cloned.1.call-done, f32[2048]{0:T(1024)S(1)} %bitcast.57, bf16[256,2048]{1,0:T(8,128)(2,1)S(1)} %copy-done.19, bf16[2048,3072]{1,0:T(8,128)(2,1)} %all-gather.17.cloned.1.call-done, f32[256,3072]{1,0:T(8,128)} %convolution_multiply_fusion.1, ...), kind=kOutput, calls=%fused_computation.16 | convolution fusion | flops 6449004544 | bytes 30429184 | tf_op jit(solution)/shard_map/dot_general | solution.py:26
  937.0 9.7 %reduce-scatter.8.cloned.1.call-done = bf16[128,2048]{1,0:T(8,128)(2,1)} async-done(((bf16[256,2048]{1,0:T(8,128)(2,1)}), bf16[128,2048]{1,0:T(8,128)(2,1)}) %reduce-scatter.8.cloned.1.call-update) | async-done | bytes 524304 | tf_op jit(solution)/shard_map/reduce_scatter | solution.py:27
  (133 shorter events, 48.0 us)
Async XLA Ops:
  6.5 52.5 %all-gather.13.cloned.1.call-start = ((), (), s32[]{:S(2)}) async-start(), calls=%async_computation.3 | async-start | bytes 1572864 | tf_op jit(solution)/shard_map/all_gather | solution.py:22
  10.0 167.3 %copy-start.20 = (f32[3072]{0:T(1024)S(1)}, f32[3072]{0:T(1024)}, u32[]{:S(2)}) copy-start(f32[3072]{0:T(1024)} %param.25) | copy-start | bytes 36868
  10.0 167.3 %all-gather.15.cloned.1.call-start = ((), (), s32[]{:S(2)}) async-start(), calls=%async_computation.4 | async-start | bytes 13369344 | tf_op jit(solution)/shard_map/all_gather | solution.py:132
  12.4 317.3 %all-gather.17.cloned.1.call-start = ((), (), s32[]{:S(2)}) async-start(), calls=%async_computation.5 | async-start | bytes 13369344 | tf_op jit(solution)/shard_map/all_gather | solution.py:133
  13.5 512.4 %all-gather.19.cloned.1.call-start = ((), (), s32[]{:S(2)}) async-start(), calls=%async_computation.6 | async-start | bytes 13369344 | tf_op jit(solution)/shard_map/all_gather | solution.py:137
  16.0 533.8 %reduce-scatter.4.cloned.1.call-start = ((), (), s32[]{:S(2)}) async-start(), calls=%async_computation.7 | async-start | bytes 1572864 | tf_op jit(solution)/shard_map/reduce_scatter | solution.py:27
  59.0 466.9 %copy-start.14 = (f32[16,1,128]{2,1,0:T(1,128)}, f32[16,1,128]{2,1,0:T(1,128)S(1)}, u32[]{:S(2)}) copy-start(f32[16,1,128]{2,1,0:T(1,128)S(1)} %all-gather) | copy-start | bytes 24580
  59.0 466.9 %copy-start.22 = (f32[3072]{0:T(1024)S(1)}, f32[3072]{0:T(1024)}, u32[]{:S(2)}) copy-start(f32[3072]{0:T(1024)} %param.27) | copy-start | bytes 36868
  59.0 466.9 %copy-start.18 = (bf16[256,2048]{1,0:T(8,128)(2,1)S(1)}, bf16[256,2048]{1,0:T(8,128)(2,1)}, u32[]{:S(2)}) copy-start(bf16[256,2048]{1,0:T(8,128)(2,1)} %all-gather.13.cloned.1.call-done) | copy-start | bytes 3145732
  525.9 23.9 %copy-start = (bf16[128,2048]{1,0:T(8,128)(2,1)S(1)}, bf16[128,2048]{1,0:T(8,128)(2,1)}, u32[]{:S(2)}) copy-start(bf16[128,2048]{1,0:T(8,128)(2,1)} %param.20) | copy-start | bytes 1572868
  525.9 25.2 %copy-start.12 = (f32[2048]{0:T(1024)S(1)}, f32[2048]{0:T(1024)}, u32[]{:S(2)}) copy-start(f32[2048]{0:T(1024)} %param.22) | copy-start | bytes 24580
  543.1 95.3 %copy-start.24 = (f32[1024]{0:T(1024)S(1)}, f32[1024]{0:T(1024)}, u32[]{:S(2)}) copy-start(f32[1024]{0:T(1024)} %param.31) | copy-start | bytes 12292
  543.1 86.1 %all-gather.25.cloned.1.call-start = ((), (), s32[]{:S(2)}) async-start(), calls=%async_computation.10 | async-start | bytes 4456448 | tf_op jit(solution)/shard_map/all_gather | solution.py:149
  543.9 94.5 %all-gather.21.cloned.1.call-start = ((), (), s32[]{:S(2)}) async-start(), calls=%async_computation.8 | async-start | bytes 1572864 | tf_op jit(solution)/shard_map/all_gather | solution.py:22
  552.2 165.8 %all-gather.27.cloned.1.call-start = ((), (), s32[]{:S(2)}) async-start(), calls=%async_computation.11 | async-start | bytes 4456448 | tf_op jit(solution)/shard_map/all_gather | solution.py:150
  553.0 242.0 %all-gather.23.cloned.1.call-start = ((), (), s32[]{:S(2)}) async-start(), calls=%async_computation.9 | async-start | bytes 4456448 | tf_op jit(solution)/shard_map/all_gather | solution.py:151
  553.9 331.1 %all-gather.29.cloned.1.call-start = ((), (), s32[]{:S(2)}) async-start(), calls=%async_computation.12 | async-start | bytes 4456448 | tf_op jit(solution)/shard_map/all_gather | solution.py:159
  554.7 341.5 %reduce-scatter.6.cloned.1.call-start = ((), (), s32[]{:S(2)}) async-start(), calls=%async_computation.13 | async-start | bytes 1572864 | tf_op jit(solution)/shard_map/reduce_scatter | solution.py:27
  598.0 120.0 %copy-start.25 = (f32[1024]{0:T(1024)S(1)}, f32[1024]{0:T(1024)}, u32[]{:S(2)}) copy-start(f32[1024]{0:T(1024)} %param.33) | copy-start | bytes 12292
  644.9 150.1 %copy-start.26 = (f32[1024]{0:T(1024)S(1)}, f32[1024]{0:T(1024)}, u32[]{:S(2)}) copy-start(f32[1024]{0:T(1024)} %param.35) | copy-start | bytes 12292
  884.9 25.0 %copy-start.21 = (f32[3072]{0:T(1024)S(1)}, f32[3072]{0:T(1024)}, u32[]{:S(2)}) copy-start(f32[3072]{0:T(1024)} %param.25) | copy-start | bytes 36868
  889.4 20.5 %all-gather.31.cloned.1.call-start = ((), (), s32[]{:S(2)}) async-start(), calls=%async_computation.14 | async-start | bytes 1572864 | tf_op jit(solution)/shard_map/all_gather | solution.py:22
  899.6 47.2 %reduce-scatter.8.cloned.1.call-start = ((), (), s32[]{:S(2)}) async-start(), calls=%async_computation.15 | async-start | bytes 1572864 | tf_op jit(solution)/shard_map/reduce_scatter | solution.py:27
  920.0 26.8 %copy-start.1 = (bf16[128,2048]{1,0:T(8,128)(2,1)S(1)}, bf16[128,2048]{1,0:T(8,128)(2,1)}, u32[]{:S(2)}) copy-start(bf16[128,2048]{1,0:T(8,128)(2,1)} %reduce-scatter.6.cloned.1.call-done) | copy-start | bytes 1572868
  (16 other events, 173.9 us)
Sparse Core Ops, SparseCore 0:
  10.1 11.7 all-gather.12
  24.6 152.6 all-gather.14
  180.1 149.5 all-gather.16
  332.2 193.6 all-gather.18
  543.2 6.5 reduce-scatter.3
  552.4 76.7 all-gather.24
  630.8 7.6 all-gather.20
  641.2 76.7 all-gather.26
  720.8 74.1 all-gather.22
  797.5 87.3 all-gather.28
  889.6 6.5 reduce-scatter.5
  899.7 10.2 all-gather.30
  937.1 9.5 reduce-scatter.7
where the time goes:
time: 956 us; the launch traced here: 955 us
  waiting for transfers between devices  732 us (77%)
  blocking collectives  84.1 us (9%)
  matrix products  83.2 us (9%)
  other arithmetic  32.5 us (3%)
  between operations  13.6 us (1%)
    all_gather x1, waiting for transfers between devices, body(): lax.all_gather(down_weight.astype(jnp.bfloat16), 'fs', axis=1, tiled=True)  196 us
    all_gather x1, waiting for transfers between devices, body(): lax.all_gather(up_part, 'fs', axis=0, tiled=True)  142 us
    all_gather x1, waiting for transfers between devices, body(): lax.all_gather(gate_part, 'fs', axis=0, tiled=True)  118 us
    all_gather x1, waiting for transfers between devices, body(): lax.all_gather(projections[1], 'fs', axis=0, tiled=True)  73.1 us
    all_gather x1, waiting for transfers between devices, body(): lax.all_gather(projections[2], 'fs', axis=0, tiled=True)  69.6 us
    all_gather x1, waiting for transfers between devices, body(): lax.all_gather(output_weight.astype(jnp.bfloat16), 'fs', axis=1, tiled=True)  59.4 us
    all_gather x1, blocking collectives, body(): lax.all_gather(down_scale, 'fs', axis=0, tiled=True)  43 us
    all_gather x1, blocking collectives, body(): lax.all_gather(output_scale, 'fs', axis=0, tiled=True)  41.1 us
  transfers between devices with their start and end apart: 13, of which 12 were waited for; matrix products, arithmetic and copies ran while one was open for 7% of the time, Pallas kernels for 0%

commit v1 on v0

--- a/solution.py
+++ b/solution.py
@@ -2,6 +2,7 @@
 import jax.numpy as jnp
 from jax import lax
 from jax.sharding import PartitionSpec as P
+from jax.lax import all_gather
 
 HEADS = 8
 HEAD_DIM = 256
@@ -10,6 +11,7 @@
 HEAD_FLOOR = 0.25
 ROTARY_BASE = 10000.0
 HIGHEST = lax.Precision.HIGHEST
+positions_define = lambda base_x: jnp.concatenate(all_gather(base_x, "fs"), 1)
 
 
 def normalize(sequence_rows, gain_vector):
@@ -156,7 +158,7 @@
             for member in range(3)
         )
     )
-    output_full = lax.all_gather(output_weight.astype(jnp.bfloat16), "fs", axis=1, tiled=True)
+    output_full = positions_define(output_weight.astype(jnp.bfloat16))
     length = mixer_input.shape[0]
     heads_local = local_width // HEAD_DIM
     decay_rates = head_rates(lax.axis_index("tp") * heads_local, heads_local, length)

time: 956 us -> 975 us (1.020)
  waiting for transfers between devices: 732 us -> 742 us
    all_gather x1, waiting for transfers between devices: 31.3 us -> 70.6 us  [body(): lax.all_gather(projections[0], 'fs', axis=0, tiled=True)]
    all_gather x1, waiting for transfers between devices: 59.4 us -> 30.9 us  [all_gather(base_x, 'fs')]
  transfers between devices with their start and end apart: 13 -> 13, of which waited for: 12 -> 12; matrix products, arithmetic and copies ran while one was open for 7% -> 4% of each run, Pallas kernels for 0% -> 0%
where the time goes in v1:
time: 975 us; the launch traced here: 974 us
  waiting for transfers between devices  742 us (76%)
  blocking collectives  85.4 us (9%)
  matrix products  83.9 us (9%)
  other arithmetic  34.3 us (4%)
  local copies, waits for them, and re-layouts  14.3 us (1%)
  between operations  13.6 us (1%)
    all_gather x1, waiting for transfers between devices, body(): lax.all_gather(down_weight.astype(jnp.bfloat16), 'fs', axis=1, tiled=True)  196 us
    all_gather x1, waiting for transfers between devices, body(): lax.all_gather(up_part, 'fs', axis=0, tiled=True)  142 us
    all_gather x1, waiting for transfers between devices, body(): lax.all_gather(gate_part, 'fs', axis=0, tiled=True)  118 us
    all_gather x1, waiting for transfers between devices, body(): lax.all_gather(projections[1], 'fs', axis=0, tiled=True)  73.1 us
    all_gather x1, waiting for transfers between devices, body(): lax.all_gather(projections[0], 'fs', axis=0, tiled=True)  70.6 us
    all_gather x1, waiting for transfers between devices, body(): lax.all_gather(projections[2], 'fs', axis=0, tiled=True)  69.4 us
    all_gather x1, blocking collectives, body(): lax.all_gather(down_scale, 'fs', axis=0, tiled=True)  43 us
    all_gather x1, blocking collectives, body(): lax.all_gather(output_scale, 'fs', axis=0, tiled=True)  42.4 us
  transfers between devices with their start and end apart: 13, of which 12 were waited for; matrix products, arithmetic and copies ran while one was open for 4% of the time, Pallas kernels for 0%

profile of v1, /device:TPU:0, one launch (start us, length us, event | category | flops | bytes accessed | tf_op | source)
XLA Modules:
  0.0 974.5 jit_solution(3764712087428823473)
XLA Ops:
  16.1 43.0 %all-gather.1 = f32[16,1,128]{2,1,0:T(1,128)S(1)} all-gather(f32[1,1,128]{2,1,0:T(1,128)S(1)} %bitcast.59), channel_id=1, replica_groups=mesh['fs'=16,'tp'=2] {'fs'}, dimensions={0}, use_global_device_ids=true | all-gather | bytes 8704 | tf_op jit(solution)/shard_map/all_gather | solution.py:129
  59.1 118.2 %all-gather.16.cloned.1.call-done = bf16[2048,3072]{1,0:T(8,128)(2,1)} async-done(((bf16[128,3072]{1,0:T(8,128)(2,1)}), bf16[2048,3072]{1,0:T(8,128)(2,1)}) %all-gather.16.cloned.1.call-update) | async-done | bytes 12582928 | tf_op jit(solution)/shard_map/all_gather | solution.py:134
  177.3 9.9 %convolution_multiply_fusion.3 = f32[256,3072]{1,0:T(8,128)} fusion(bf16[256,2048]{1,0:T(8,128)(2,1)} %all-gather.14.cloned.1.call-done, bf16[2048,3072]{1,0:T(8,128)(2,1)} %all-gather.16.cloned.1.call-done, f32[3072]{0:T(1024)S(1)} %copy-done.17), kind=kOutput, calls=%fused_computation.7 | convolution fusion | flops 3222011904 | bytes 16789504 | tf_op jit(solution)/shard_map/dot_general | solution.py:137
  187.2 142.5 %all-gather.18.cloned.1.call-done = bf16[2048,3072]{1,0:T(8,128)(2,1)} async-done(((bf16[128,3072]{1,0:T(8,128)(2,1)}), bf16[2048,3072]{1,0:T(8,128)(2,1)}) %all-gather.18.cloned.1.call-update) | async-done | bytes 12582928 | tf_op jit(solution)/shard_map/all_gather | solution.py:135
  329.7 196.2 %all-gather.20.cloned.1.call-done = bf16[3072,2048]{1,0:T(8,128)(2,1)} async-done(((bf16[3072,128]{1,0:T(8,128)(2,1)}), bf16[3072,2048]{1,0:T(8,128)(2,1)}) %all-gather.20.cloned.1.call-update) | async-done | bytes 12582928 | tf_op jit(solution)/shard_map/all_gather | solution.py:139
  525.9 17.1 %fusion.6 = bf16[256,2048]{1,0:T(8,128)(2,1)} fusion(bf16[3072,2048]{1,0:T(8,128)(2,1)} %all-gather.20.cloned.1.call-done, f32[2048]{0:T(1024)S(1)} %bitcast.56, bf16[256,2048]{1,0:T(8,128)(2,1)S(1)} %copy-done.15, bf16[2048,3072]{1,0:T(8,128)(2,1)} %all-gather.18.cloned.1.call-done, f32[256,3072]{1,0:T(8,128)} %convolution_multiply_fusion.3, ...), kind=kOutput, calls=%fused_computation.15 | convolution fusion | flops 6449004544 | bytes 30429184 | tf_op jit(solution)/shard_map/dot_general | solution.py:28
  544.8 5.0 reduce-scatter.4.cloned.1.call-done
  553.9 42.4 %all-gather.2 = f32[16,1,128]{2,1,0:T(1,128)} all-gather(f32[1,1,128]{2,1,0:T(1,128)S(1)} %bitcast.60), channel_id=1, replica_groups=mesh['fs'=16,'tp'=2] {'fs'}, dimensions={0}, use_global_device_ids=true | all-gather | bytes 8704 | tf_op jit(solution)/shard_map/all_gather | solution.py:130
  598.4 30.9 %all-gather.32.cloned.1.call-done = bf16[16384,128]{1,0:T(8,128)(2,1)} async-done(((bf16[1024,128]{1,0:T(8,128)(2,1)}), bf16[16384,128]{1,0:T(8,128)(2,1)}) %all-gather.32.cloned.1.call-update) | async-done | bytes 4194320 | tf_op jit(solution)/shard_map/all_gather | solution.py:14
  629.3 6.4 copy.61
  635.7 70.6 %all-gather.26.cloned.1.call-done = bf16[2048,1024]{1,0:T(8,128)(2,1)} async-done(((bf16[128,1024]{1,0:T(8,128)(2,1)}), bf16[2048,1024]{1,0:T(8,128)(2,1)}) %all-gather.26.cloned.1.call-update) | async-done | bytes 4194320 | tf_op jit(solution)/shard_map/all_gather | solution.py:151
  706.3 9.2 all-gather.22.cloned.1.call-done
  715.5 4.8 convolution_multiply_fusion.8
  721.9 73.1 %all-gather.28.cloned.1.call-done = bf16[2048,1024]{1,0:T(8,128)(2,1)} async-done(((bf16[128,1024]{1,0:T(8,128)(2,1)}), bf16[2048,1024]{1,0:T(8,128)(2,1)}) %all-gather.28.cloned.1.call-update) | async-done | bytes 4194320 | tf_op jit(solution)/shard_map/all_gather | solution.py:152
  795.0 4.7 convolution_multiply_fusion.7
  802.4 69.4 %all-gather.24.cloned.1.call-done = bf16[2048,1024]{1,0:T(8,128)(2,1)} async-done(((bf16[128,1024]{1,0:T(8,128)(2,1)}), bf16[2048,1024]{1,0:T(8,128)(2,1)}) %all-gather.24.cloned.1.call-update) | async-done | bytes 4194320 | tf_op jit(solution)/shard_map/all_gather | solution.py:153
  871.9 4.6 fusion.10
  884.4 10.4 %while.13 = (s32[]{:T(128)}, f32[4,256,256]{2,1,0:T(8,128)S(1)}, f32[4,4,256,256]{3,2,1,0:T(8,128)}, f32[4,4,256,256]{3,2,1,0:T(8,128)}, s32[]{:T(128)}, /*index=5*/s32[]{:T(128)}, s32[]{:T(128)}) while((s32[]{:T(128)}, f32[4,256,256]{2,1,0:T(8,128)S(1)}, f32[4,4,256,256]{3,2,1,0:T(8,128)}, f32[4,4,256,256]{3,2,1,0:T(8,128)}, ...), condition=%wide.region_4.5_spmd.clone, body=%wide.region_3.4_spmd.clone.sunk | while | flops 1048603 | bytes 5243520 | solution.py:93
  894.8 5.2 fusion.24
  908.2 7.1 reduce-scatter.6.cloned.1.call-done
  919.0 10.1 %all-gather.30.cloned.1.call-done = bf16[256,2048]{1,0:T(8,128)(2,1)} async-done(((bf16[128,2048]{1,0:T(8,128)(2,1)}), bf16[256,2048]{1,0:T(8,128)(2,1)}) %all-gather.30.cloned.1.call-update) | async-done | bytes 1048592 | tf_op jit(solution)/shard_map/all_gather | solution.py:24
  929.1 10.0 %convolution_multiply_fusion.1 = f32[256,3072]{1,0:T(8,128)} fusion(bf16[256,2048]{1,0:T(8,128)(2,1)} %all-gather.30.cloned.1.call-done, bf16[2048,3072]{1,0:T(8,128)(2,1)} %all-gather.16.cloned.1.call-done, f32[3072]{0:T(1024)S(1)} %copy-done.18), kind=kOutput, calls=%fused_computation.5 | convolution fusion | flops 3222011904 | bytes 16789504 | tf_op jit(solution)/shard_map/dot_general | solution.py:174
  939.1 17.0 %fusion.7 = bf16[256,2048]{1,0:T(8,128)(2,1)} fusion(bf16[3072,2048]{1,0:T(8,128)(2,1)} %all-gather.20.cloned.1.call-done, f32[2048]{0:T(1024)S(1)} %bitcast.57, bf16[256,2048]{1,0:T(8,128)(2,1)S(1)} %copy-done.16, bf16[2048,3072]{1,0:T(8,128)(2,1)} %all-gather.18.cloned.1.call-done, f32[256,3072]{1,0:T(8,128)} %convolution_multiply_fusion.1, ...), kind=kOutput, calls=%fused_computation.16 | convolution fusion | flops 6449004544 | bytes 30429184 | tf_op jit(solution)/shard_map/dot_general | solution.py:28
  956.2 9.7 reduce-scatter.8.cloned.1.call-done
  (126 shorter events, 53.8 us)
Async XLA Ops:
  6.5 52.6 %all-gather.14.cloned.1.call-start = ((), (), s32[]{:S(2)}) async-start(), calls=%async_computation.3 | async-start | bytes 1572864 | tf_op jit(solution)/shard_map/all_gather | solution.py:24
  10.0 167.3 %copy-start.17 = (f32[3072]{0:T(1024)S(1)}, f32[3072]{0:T(1024)}, u32[]{:S(2)}) copy-start(f32[3072]{0:T(1024)} %param.25) | copy-start | bytes 36868
  10.0 167.3 %all-gather.16.cloned.1.call-start = ((), (), s32[]{:S(2)}) async-start(), calls=%async_computation.4 | async-start | bytes 13369344 | tf_op jit(solution)/shard_map/all_gather | solution.py:134
  12.5 317.2 %all-gather.18.cloned.1.call-start = ((), (), s32[]{:S(2)}) async-start(), calls=%async_computation.5 | async-start | bytes 13369344 | tf_op jit(solution)/shard_map/all_gather | solution.py:135
  13.6 512.3 %all-gather.20.cloned.1.call-start = ((), (), s32[]{:S(2)}) async-start(), calls=%async_computation.6 | async-start | bytes 13369344 | tf_op jit(solution)/shard_map/all_gather | solution.py:139
  16.1 533.7 %reduce-scatter.4.cloned.1.call-start = ((), (), s32[]{:S(2)}) async-start(), calls=%async_computation.7 | async-start | bytes 1572864 | tf_op jit(solution)/shard_map/reduce_scatter | solution.py:29
  59.1 466.8 %copy-start.19 = (f32[3072]{0:T(1024)S(1)}, f32[3072]{0:T(1024)}, u32[]{:S(2)}) copy-start(f32[3072]{0:T(1024)} %param.27) | copy-start | bytes 36868
  59.1 466.8 %copy-start.15 = (bf16[256,2048]{1,0:T(8,128)(2,1)S(1)}, bf16[256,2048]{1,0:T(8,128)(2,1)}, u32[]{:S(2)}) copy-start(bf16[256,2048]{1,0:T(8,128)(2,1)} %all-gather.14.cloned.1.call-done) | copy-start | bytes 3145732
  525.9 18.0 %copy-start.5 = (f32[128,1024]{1,0:T(8,128)S(1)}, f32[128,1024]{1,0:T(8,128)}, u32[]{:S(2)}) copy-start(f32[128,1024]{1,0:T(8,128)} %param.30) | copy-start | bytes 1572868
  525.9 23.9 %copy-start = (bf16[128,2048]{1,0:T(8,128)(2,1)S(1)}, bf16[128,2048]{1,0:T(8,128)(2,1)}, u32[]{:S(2)}) copy-start(bf16[128,2048]{1,0:T(8,128)(2,1)} %param.20) | copy-start | bytes 1572868
  543.0 86.2 %all-gather.32.cloned.1.call-start = ((), (), s32[]{:S(2)}) async-start(), calls=%async_computation.15 | async-start | bytes 4456448 | tf_op jit(solution)/shard_map/all_gather | solution.py:14
  543.9 162.4 %all-gather.26.cloned.1.call-start = ((), (), s32[]{:S(2)}) async-start(), calls=%async_computation.10 | async-start | bytes 4456448 | tf_op jit(solution)/shard_map/all_gather | solution.py:151
  544.7 170.7 %all-gather.22.cloned.1.call-start = ((), (), s32[]{:S(2)}) async-start(), calls=%async_computation.8 | async-start | bytes 1572864 | tf_op jit(solution)/shard_map/all_gather | solution.py:24
  552.2 242.9 %all-gather.28.cloned.1.call-start = ((), (), s32[]{:S(2)}) async-start(), calls=%async_computation.11 | async-start | bytes 4456448 | tf_op jit(solution)/shard_map/all_gather | solution.py:152
  553.0 318.9 %all-gather.24.cloned.1.call-start = ((), (), s32[]{:S(2)}) async-start(), calls=%async_computation.9 | async-start | bytes 4456448 | tf_op jit(solution)/shard_map/all_gather | solution.py:153
  553.8 361.5 %reduce-scatter.6.cloned.1.call-start = ((), (), s32[]{:S(2)}) async-start(), calls=%async_computation.12 | async-start | bytes 1572864 | tf_op jit(solution)/shard_map/reduce_scatter | solution.py:29
  629.3 86.2 %copy-start.21 = (f32[1024]{0:T(1024)S(1)}, f32[1024]{0:T(1024)}, u32[]{:S(2)}) copy-start(f32[1024]{0:T(1024)} %param.31) | copy-start | bytes 12292
  635.7 159.3 %copy-start.22 = (f32[1024]{0:T(1024)S(1)}, f32[1024]{0:T(1024)}, u32[]{:S(2)}) copy-start(f32[1024]{0:T(1024)} %param.33) | copy-start | bytes 12292
  721.9 150.0 %copy-start.23 = (f32[1024]{0:T(1024)S(1)}, f32[1024]{0:T(1024)}, u32[]{:S(2)}) copy-start(f32[1024]{0:T(1024)} %param.35) | copy-start | bytes 12292
  903.7 25.4 %copy-start.18 = (f32[3072]{0:T(1024)S(1)}, f32[3072]{0:T(1024)}, u32[]{:S(2)}) copy-start(f32[3072]{0:T(1024)} %param.25) | copy-start | bytes 36868
  908.2 20.9 %all-gather.30.cloned.1.call-start = ((), (), s32[]{:S(2)}) async-start(), calls=%async_computation.13 | async-start | bytes 1572864 | tf_op jit(solution)/shard_map/all_gather | solution.py:24
  918.7 20.4 %copy-start.20 = (f32[3072]{0:T(1024)S(1)}, f32[3072]{0:T(1024)}, u32[]{:S(2)}) copy-start(f32[3072]{0:T(1024)} %param.27) | copy-start | bytes 36868
  918.7 47.2 %reduce-scatter.8.cloned.1.call-start = ((), (), s32[]{:S(2)}) async-start(), calls=%async_computation.14 | async-start | bytes 1572864 | tf_op jit(solution)/shard_map/reduce_scatter | solution.py:29
  939.1 26.8 %copy-start.1 = (bf16[128,2048]{1,0:T(8,128)(2,1)S(1)}, bf16[128,2048]{1,0:T(8,128)(2,1)}, u32[]{:S(2)}) copy-start(bf16[128,2048]{1,0:T(8,128)(2,1)} %reduce-scatter.6.cloned.1.call-done) | copy-start | bytes 1572868
  (13 other events, 104.9 us)
Sparse Core Ops, SparseCore 0:
  10.1 11.7 all-gather.13
  24.6 152.6 all-gather.15
  180.1 149.5 all-gather.17
  332.2 193.6 all-gather.19
  543.2 6.5 reduce-scatter.3
  552.4 76.8 all-gather.31
  632.0 74.1 all-gather.25
  707.8 7.6 all-gather.21
  718.2 76.7 all-gather.27
  797.6 74.1 all-gather.23
  908.3 6.9 reduce-scatter.5
  918.8 10.2 all-gather.29
  956.3 9.5 reduce-scatter.7
